TPU v7x, 32 devices: a whole 2x2x4 slice. The times are simulated.
32 devices in a mesh: sp: 8 (over z, y), tp: 4 (over x, core).
Axes of the slice: x: 2, y: 2, z: 4, core: 2. Of those that a mesh axis runs over, the one named last changes fastest.
Arguments:
- queries: bfloat16 [3072, 2048], P('sp', 'tp'), may hold values from -200 to 200
- keys: bfloat16 [3072, 2048], P('sp', 'tp'), may hold values from -200 to 200
- values: bfloat16 [3072, 2048], P('sp', 'tp'), may hold values from -6 to 6
- forget_sums: float32 [3072, 16], P('sp', 'tp'), may hold values from -3072 to 0, as said below
- residual_in: bfloat16 [3072, 2048], P(('sp', 'tp')), may hold values from -0.59765625 to 0.59765625
- out_weight: bfloat16 [2048, 2048], P('tp'), may hold values from -0.125 to 0.125
- norm_gain: bfloat16 [2048], replicated, may hold values from 0.099609375 to 1.8984375
- gate_weight: bfloat16 [2048, 3072], P('sp', 'tp'), may hold values from -0.125 to 0.125
- up_weight: bfloat16 [2048, 3072], P('sp', 'tp'), may hold values from -0.125 to 0.125
- down_weight: bfloat16 [3072, 2048], P('tp', 'sp'), may hold values from -0.109375 to 0.109375
Outputs:
- mixed: bfloat16 [3072, 2048], P(('sp', 'tp'))
Inputs may be any that keep to these rules, and one draw needn't show every extreme that they name: `forget_sums`: in every head the entries never rise from one position to the next.
All inputs are finite; a program needn't handle non-finite values.
Results may differ from a plain program's by a relative error of at most 0.022.
Values may be sent and summed in bfloat16 or wider, within the bound.
A program may use at most 192 MiB of HBM per device.

v0:
```python
import math

import jax
import jax.numpy as jnp
from jax import lax
from jax.sharding import PartitionSpec as P

HD = 128


def attend_block(carried, block, query_rows, query_gate, query_pos, heads_here):
    row_top, row_total, weighted = carried
    key_rows, value_rows, key_gate, key_pos = block
    score_scale = HD ** (-0.5)
    tops, totals, sums = ([], [], [])
    for head_index in range(heads_here):
        columns = slice(head_index * HD, (head_index + 1) * HD)
        scores = (
            jnp.einsum(
                "qd,kd->qk",
                query_rows[:, columns],
                key_rows[:, columns],
                preferred_element_type=jnp.float32,
            )
            * score_scale
        )
        scores = scores + query_gate[:, head_index : head_index + 1] - key_gate[None, :, head_index]
        scores = jnp.where(key_pos[None, :] <= query_pos[:, None], scores, -jnp.inf)
        new_top = jnp.maximum(row_top[:, head_index], jnp.max(scores, axis=1))
        shrink = jnp.exp(row_top[:, head_index] - new_top)
        expon = jnp.exp(scores - new_top[:, None])
        totals.append(shrink * row_total[:, head_index] + jnp.sum(expon, axis=1))
        sums.append(
            shrink[:, None] * weighted[:, columns]
            + jnp.dot(
                expon.astype(jnp.bfloat16),
                value_rows[:, columns],
                preferred_element_type=jnp.float32,
            )
        )
        tops.append(new_top)
    return (jnp.stack(tops, axis=1), jnp.stack(totals, axis=1), jnp.concatenate(sums, axis=1))


def shards(
    queries,
    keys,
    values,
    forget_sums,
    residual_in,
    out_weight,
    norm_gain,
    gate_weight,
    up_weight,
    down_weight,
):
    rows_here = queries.shape[0]
    heads_here = queries.shape[1] // HD
    first = lax.axis_index("sp") * rows_here
    query_pos = first + jnp.arange(rows_here, dtype=jnp.int32)
    early_gate, early_up = (
        lax.all_gather(gate_weight, "sp", axis=0, tiled=True),
        lax.all_gather(up_weight, "sp", axis=0, tiled=True),
    )
    all_gates = lax.all_gather(forget_sums, "sp", axis=0, tiled=True)
    start_state = (
        jnp.full((rows_here, heads_here), -1e30, jnp.float32),
        jnp.zeros((rows_here, heads_here), jnp.float32),
        jnp.zeros((rows_here, heads_here * HD), jnp.float32),
    )
    carried = start_state
    key_rows = lax.all_gather(keys, "sp", axis=0, tiled=True)
    value_rows = lax.all_gather(values, "sp", axis=0, tiled=True)
    count = key_rows.shape[0]
    block_rows = math.gcd(count, 512)
    block_count = count // block_rows
    key_pos = jnp.arange(count, dtype=jnp.int32)
    blocks = (
        key_rows.reshape(block_count, block_rows, -1),
        value_rows.reshape(block_count, block_rows, -1),
        all_gates.reshape(block_count, block_rows, -1),
        key_pos.reshape(block_count, block_rows),
    )

    def advance(inner, block):
        return (attend_block(inner, block, queries, forget_sums, query_pos, heads_here), None)

    carried, unused = lax.scan(advance, carried, blocks)
    row_top, row_total, weighted = carried
    attended = (weighted / jnp.repeat(row_total, HD, axis=1)).astype(jnp.bfloat16)
    projected = lax.psum_scatter(
        jnp.dot(attended, out_weight, preferred_element_type=jnp.float32).astype(jnp.bfloat16),
        "tp",
        scatter_dimension=0,
        tiled=True,
    ).astype(jnp.float32)
    stream = residual_in.astype(jnp.float32) + projected
    normed = stream * lax.rsqrt(jnp.mean(stream * stream, axis=1, keepdims=True) + 1e-06)
    normed = (normed * norm_gain.astype(jnp.float32)).astype(jnp.bfloat16)
    every_row = lax.all_gather(normed, "tp", axis=0, tiled=True)
    gate = jnp.dot(every_row, early_gate, preferred_element_type=jnp.float32)
    up = jnp.dot(every_row, early_up, preferred_element_type=jnp.float32)
    hidden = (jax.nn.silu(gate) * up).astype(jnp.bfloat16)
    partial_value = jnp.dot(
        hidden,
        lax.all_gather(down_weight, "sp", axis=1, tiled=True),
        preferred_element_type=jnp.float32,
    ).astype(jnp.bfloat16)
    summed = lax.psum_scatter(
        partial_value.astype(jnp.float32).astype(jnp.bfloat16),
        "tp",
        scatter_dimension=0,
        tiled=True,
    ).astype(jnp.float32)
    return (stream + summed).astype(jnp.bfloat16)


def solution(mesh):
    placed = (
        P("sp", "tp"),
        P("sp", "tp"),
        P("sp", "tp"),
        P("sp", "tp"),
        P(("sp", "tp"), None),
        P("tp", None),
        P(),
        P("sp", "tp"),
        P("sp", "tp"),
        P("tp", "sp"),
    )
    return jax.shard_map(
        shards, mesh=mesh, in_specs=placed, out_specs=P(("sp", "tp"), None), check_vma=False
    )
```

profile of v0, /device:TPU:9, one launch (start us, length us, event | category | flops | bytes accessed | tf_op | source)
XLA Modules:
  0.0 440.0 jit_solution(3732854181924096891)
XLA Ops:
  6.5 0.7 all-gather.7.cloned.1.call-update
  7.3 0.7 all-gather.9.cloned.1.call-update
  8.1 23.1 %all_gather.22 = f32[3072,4]{0,1:T(4,128)S(1)} all-gather(f32[384,4]{0,1:T(4,128)} %param.15), channel_id=1, replica_groups=mesh['sp'=8,'tp'=4] {'sp'}, dimensions={0}, use_global_device_ids=true | all-gather | bytes 55296 | tf_op jit(solution)/shard_map/all_gather | solution.py:65
  31.2 38.2 %all-gather.7.cloned.1.call-done = bf16[3072,512]{1,0:T(8,128)(2,1)} async-done(((bf16[384,512]{1,0:T(8,128)(2,1)}), bf16[3072,512]{1,0:T(8,128)(2,1)}) %all-gather.7.cloned.1.call-update) | async-done | bytes 3145744 | tf_op jit(solution)/shard_map/all_gather | solution.py:72
  69.5 60.9 %all-gather.9.cloned.1.call-done = bf16[3072,512]{1,0:T(8,128)(2,1)} async-done(((bf16[384,512]{1,0:T(8,128)(2,1)}), bf16[3072,512]{1,0:T(8,128)(2,1)}) %all-gather.9.cloned.1.call-update) | async-done | bytes 3145744 | tf_op jit(solution)/shard_map/all_gather | solution.py:73
  130.5 28.8 %while.15 = (s32[]{:T(128)}, f32[384,4]{0,1:T(4,128)S(1)}, f32[384,4]{0,1:T(4,128)S(1)}, f32[384,512]{0,1:T(8,128)S(1)}, s32[6,512]{1,0:T(8,128)S(1)}, /*index=5...) while((s32[]{:T(128)}, f32[384,4]{0,1:T(4,128)S(1)}, ...), condition=%wide.region_9.10_spmd.clone, body=%wide.region_0.9_spmd.clone.sunk | while | flops 411514752 | bytes 16326277 | solution.py:88
  130.5 1.3 dynamic-slice_bitcast_fusion.6
  131.8 0.3 fusion.90
  132.2 0.3 fusion.91
  132.5 0.3 fusion.92
  132.9 0.3 fusion.93
  133.3 0.3 convolution_add_fusion.11
  133.9 0.3 convolution_add_fusion.9
  134.2 0.3 convolution_add_fusion.8
  135.3 1.3 dynamic-slice_bitcast_fusion.6
  136.7 0.3 fusion.90
  137.0 0.3 fusion.91
  137.4 0.3 fusion.92
  137.7 0.3 fusion.93
  138.7 0.3 convolution_add_fusion.9
  139.0 0.3 convolution_add_fusion.8
  140.1 1.3 dynamic-slice_bitcast_fusion.6
  141.5 0.3 fusion.90
  141.8 0.3 fusion.91
  142.2 0.3 fusion.92
  142.5 0.3 fusion.93
  143.5 0.3 convolution_add_fusion.9
  143.8 0.3 convolution_add_fusion.8
  144.9 1.3 dynamic-slice_bitcast_fusion.6
  146.3 0.3 fusion.90
  146.6 0.3 fusion.91
  147.0 0.3 fusion.92
  147.3 0.3 fusion.93
  148.3 0.3 convolution_add_fusion.9
  148.6 0.3 convolution_add_fusion.8
  149.7 1.3 dynamic-slice_bitcast_fusion.6
  151.1 0.3 fusion.90
  151.4 0.3 fusion.91
  151.8 0.3 fusion.92
  152.1 0.3 fusion.93
  153.1 0.3 convolution_add_fusion.9
  153.4 0.3 convolution_add_fusion.8
  154.5 1.3 dynamic-slice_bitcast_fusion.6
  155.9 0.3 fusion.90
  156.2 0.3 fusion.91
  156.6 0.3 fusion.92
  156.9 0.3 fusion.93
  157.9 0.3 convolution_add_fusion.9
  158.2 0.3 convolution_add_fusion.8
  159.4 2.2 convolution_convert_fusion.1
  161.6 0.5 all-gather.13.cloned.1.call-update
  162.2 27.5 %reduce-scatter.3.cloned.1.call-done = bf16[96,2048]{1,0:T(8,128)(2,1)} async-done(((bf16[384,2048]{1,0:T(8,128)(2,1)}), bf16[96,2048]{1,0:T(8,128)(2,1)}) %reduce-scatter.3.cloned.1.call-update) | async-done | bytes 393232 | tf_op jit(solution)/shard_map/reduce_scatter | solution.py:91
  189.7 1.2 multiply_reduce_fusion
  190.9 1.9 multiply_convert_fusion
  192.9 0.5 all-gather.15.cloned.1.call-update
  193.5 0.7 all-gather.17.cloned.1.call-update
  194.2 56.3 %all-gather.13.cloned.1.call-done = bf16[2048,768]{1,0:T(8,128)(2,1)} async-done(((bf16[256,768]{1,0:T(8,128)(2,1)}), bf16[2048,768]{1,0:T(8,128)(2,1)}) %all-gather.13.cloned.1.call-update) | async-done | bytes 3145744 | tf_op jit(solution)/shard_map/all_gather | solution.py:62
  250.5 21.6 %all-gather.11.cloned.1.call-done = bf16[384,2048]{1,0:T(8,128)(2,1)} async-done(((bf16[96,2048]{1,0:T(8,128)(2,1)}), bf16[384,2048]{1,0:T(8,128)(2,1)}) %all-gather.11.cloned.1.call-update) | async-done | bytes 1572880 | tf_op jit(solution)/shard_map/all_gather | solution.py:100
  272.1 4.8 %fusion.55 = f32[384,768]{1,0:T(8,128)} fusion(bf16[384,2048]{1,0:T(8,128)(2,1)} %all-gather.11.cloned.1.call-done, bf16[2048,768]{1,0:T(8,128)(2,1)} %all-gather.13.cloned.1.call-done), kind=kOutput, calls=%fused_computation.100 | convolution fusion | flops 1207959552 | bytes 5898240 | tf_op jit(solution)/shard_map/dot_general | solution.py:101
  276.8 55.5 %all-gather.15.cloned.1.call-done = bf16[2048,768]{1,0:T(8,128)(2,1)} async-done(((bf16[256,768]{1,0:T(8,128)(2,1)}), bf16[2048,768]{1,0:T(8,128)(2,1)}) %all-gather.15.cloned.1.call-update) | async-done | bytes 3145744 | tf_op jit(solution)/shard_map/all_gather | solution.py:63
  332.3 62.3 %all-gather.17.cloned.1.call-done = bf16[768,2048]{1,0:T(8,128)(2,1)} async-done(((bf16[768,256]{1,0:T(8,128)(2,1)}), bf16[768,2048]{1,0:T(8,128)(2,1)}) %all-gather.17.cloned.1.call-update) | async-done | bytes 3145744 | tf_op jit(solution)/shard_map/all_gather | solution.py:106
  394.6 7.9 %convolution_convert_fusion = bf16[384,2048]{1,0:T(8,128)(2,1)} fusion(bf16[768,2048]{1,0:T(8,128)(2,1)} %all-gather.17.cloned.1.call-done, bf16[384,2048]{1,0:T(8,128)(2,1)} %all-gather.11.cloned.1.call-done, bf16[2048,768]{1,0:T(8,128)(2,1)} %all-gather.15.cloned.1.call-done, f32[384,768]{1,0:T(8,128)} %fusion.55), kind=kOutput, calls=%fused_computation.81 | convolution fusion | flops 2418475008 | bytes 10616832 | tf_op jit(solution)/shard_map/dot_general | solution.py:104
  402.5 28.8 %reduce-scatter.5.cloned.1.call-done = bf16[96,2048]{1,0:T(8,128)(2,1)} async-done(((bf16[384,2048]{1,0:T(8,128)(2,1)}), bf16[96,2048]{1,0:T(8,128)(2,1)}) %reduce-scatter.5.cloned.1.call-update) | async-done | bytes 393232 | tf_op jit(solution)/shard_map/reduce_scatter | solution.py:109
  431.3 1.9 add_convert_fusion
  (125 shorter events, 8.9 us)
Async XLA Ops:
  6.5 152.8 %copy-start = (bf16[512,2048]{1,0:T(8,128)(2,1)S(1)}, bf16[512,2048]{1,0:T(8,128)(2,1)}, u32[]{:S(2)}) copy-start(bf16[512,2048]{1,0:T(8,128)(2,1)} %param.17) | copy-start | bytes 6291460
  6.5 123.9 %copy-start.3 = (f32[384,4]{0,1:T(4,128)S(1)}, f32[384,4]{0,1:T(4,128)}, u32[]{:S(2)}) copy-start(f32[384,4]{0,1:T(4,128)} %param.15) | copy-start | bytes 18436
  6.5 123.9 %copy-start.5 = (bf16[384,512]{1,0:T(8,128)(2,1)S(1)}, bf16[384,512]{1,0:T(8,128)(2,1)}, u32[]{:S(2)}) copy-start(bf16[384,512]{1,0:T(8,128)(2,1)} %param.12) | copy-start | bytes 1179652
  6.5 62.9 %all-gather.7.cloned.1.call-start = ((), (), s32[]{:S(2)}) async-start(), calls=%async_computation.2 | async-start | bytes 3538944 | tf_op jit(solution)/shard_map/all_gather | solution.py:72
  7.3 123.1 %all-gather.9.cloned.1.call-start = ((), (), s32[]{:S(2)}) async-start(), calls=%async_computation.3 | async-start | bytes 3538944 | tf_op jit(solution)/shard_map/all_gather | solution.py:73
  8.0 181.7 %reduce-scatter.3.cloned.1.call-start = ((), (), s32[]{:S(2)}) async-start(), calls=%async_computation.4 | async-start | bytes 1966080 | tf_op jit(solution)/shard_map/reduce_scatter | solution.py:91
  161.5 0.7 copy-start.4
  161.5 28.2 %copy-start.1 = (bf16[96,2048]{1,0:T(8,128)(2,1)S(1)}, bf16[96,2048]{1,0:T(8,128)(2,1)}, u32[]{:S(2)}) copy-start(bf16[96,2048]{1,0:T(8,128)(2,1)} %param.16) | copy-start | bytes 1179652
  161.5 89.0 %all-gather.13.cloned.1.call-start = ((), (), s32[]{:S(2)}) async-start(), calls=%async_computation.6 | async-start | bytes 3538944 | tf_op jit(solution)/shard_map/all_gather | solution.py:62
  162.1 110.0 %all-gather.11.cloned.1.call-start = ((), (), s32[]{:S(2)}) async-start(), calls=%async_computation.5 | async-start | bytes 1966080 | tf_op jit(solution)/shard_map/all_gather | solution.py:100
  192.9 139.5 %all-gather.15.cloned.1.call-start = ((), (), s32[]{:S(2)}) async-start(), calls=%async_computation.7 | async-start | bytes 3538944 | tf_op jit(solution)/shard_map/all_gather | solution.py:63
  193.4 201.2 %all-gather.17.cloned.1.call-start = ((), (), s32[]{:S(2)}) async-start(), calls=%async_computation.8 | async-start | bytes 3538944 | tf_op jit(solution)/shard_map/all_gather | solution.py:106
  194.2 237.1 %reduce-scatter.5.cloned.1.call-start = ((), (), s32[]{:S(2)}) async-start(), calls=%async_computation.9 | async-start | bytes 1966080 | tf_op jit(solution)/shard_map/reduce_scatter | solution.py:109
  402.5 28.8 %copy-start.2 = (bf16[96,2048]{1,0:T(8,128)(2,1)S(1)}, bf16[96,2048]{1,0:T(8,128)(2,1)}, u32[]{:S(2)}) copy-start(bf16[96,2048]{1,0:T(8,128)(2,1)} %reduce-scatter.3.cloned.1.call-done) | copy-start | bytes 1179652
Sparse Core Ops, SparseCore 0:
  9.5 59.9 all-gather.6
  71.6 58.6 all-gather.8
  161.7 27.9 reduce-scatter.2
  191.7 58.7 all-gather.12
  251.9 20.1 all-gather.10
  274.1 58.1 all-gather.14
  334.4 60.1 all-gather.16
  402.6 28.6 reduce-scatter.4
where the time goes:
time: 442 us; the launch traced here: 440 us
  waiting for transfers between devices  354 us (80%)
  matrix products  30.1 us (7%)
  blocking collectives  23.1 us (5%)
  between operations  13.6 us (3%)
  other arithmetic  9.88 us (2%)
  local copies, waits for them, and re-layouts  8.11 us (2%)
    all_gather x1, waiting for transfers between devices, shards(): lax.all_gather(down_weight, 'sp', axis=1, tiled=True)  62.3 us
    all_gather x1, waiting for transfers between devices, shards(): value_rows = lax.all_gather(values, 'sp', axis=0, tiled=True)  60.9 us
    all_gather x1, waiting for transfers between devices, shards(): lax.all_gather(gate_weight, 'sp', axis=0, tiled=True)  56.3 us
    all_gather x1, waiting for transfers between devices, shards(): lax.all_gather(up_weight, 'sp', axis=0, tiled=True)  55.5 us
    all_gather x1, waiting for transfers between devices, shards(): key_rows = lax.all_gather(keys, 'sp', axis=0, tiled=True)  38.2 us
    reduce_scatter x1, waiting for transfers between devices, shards(): lax.psum_scatter(partial_value.astype(jnp.float32).astype(jnp.bfloat16),...  28.8 us
    reduce_scatter x1, waiting for transfers between devices, shards(): lax.psum_scatter(jnp.dot(attended, out_weight, preferred_element_type=jnp...  27.5 us
    all_gather x1, blocking collectives, shards(): all_gates = lax.all_gather(forget_sums, 'sp', axis=0, tiled=True)  23.1 us
  transfers between devices with their start and end apart: 8, of which 8 were waited for; matrix products, arithmetic and copies ran while one was open for 2% of the time, Pallas kernels for 0%

commit v1 on v0

v1 whole, which is shorter than its diff:
```python
import functools
import math

import jax
import jax.numpy as jnp
from jax import lax
from jax.experimental import pallas as pl
from jax.experimental.pallas import tpu as pltpu
from jax.sharding import PartitionSpec as P

HD = 128
F32 = jnp.float32
BF16 = jnp.bfloat16


def remote(src, dst, send_sem, recv_sem, **where):
    return pltpu.make_async_remote_copy(
        src_ref=src,
        dst_ref=dst,
        send_sem=send_sem,
        recv_sem=recv_sem,
        device_id=where,
        device_id_type=pl.DeviceIdType.MESH,
    )


def layer_kernel(
    n, n_tp, heads,
    q, k, v, ft, res, ow, gain, gw, uw, dw,
    out,
    qb, kb, vb, fb, ob, ab, pb, rb, st, xb, gb, ub, db, hb, p2, r2,
    local_sem, qs, qr, fs, fr, kzs, kys, kr, vzs, vys, vr,
    wus, wds, wys, wr, os_, or_, ps, pr, xs, xr, es, er,
):
    sp, tp = lax.axis_index("sp"), lax.axis_index("tp")
    n_z = heads
    n_y = n // n_z
    z, y = sp // n_y, lax.rem(sp, n_y)
    rows = q.shape[0]
    q_rows = rows // n_y
    t_rows = rows // n_tp
    width = ow.shape[1]
    up_depth = gw.shape[0]

    def head_cols(head):
        return pl.ds(pl.multiple_of(head * HD, HD), HD)

    def stripe(part):
        return pl.ds(pl.multiple_of(part * q_rows, q_rows), q_rows)

    def tp_rows(part):
        return pl.ds(pl.multiple_of(part * t_rows, t_rows), t_rows)

    sends = []

    def go(copy):
        copy.start()
        sends.append(copy)

    own = [
        (k.at[:, head_cols(z)], kb.at[sp]),
        (v.at[:, head_cols(z)], vb.at[sp]),
        (q.at[stripe(y), head_cols(z)], qb.at[sp]),
        (ft, fb.at[sp]),
        (gw, gb.at[pl.ds(pl.multiple_of(sp * up_depth, up_depth), up_depth)]),
        (uw, ub.at[pl.ds(pl.multiple_of(sp * up_depth, up_depth), up_depth)]),
        (dw, db.at[sp]),
    ]
    own = [pltpu.make_async_copy(a, b, local_sem.at[i]) for i, (a, b) in enumerate(own)]
    for copy in own:
        copy.start()
    for off in range(1, n_z):
        dz = lax.rem(z + off, n_z)
        for src, buf, ss, rs in ((k, kb, kzs, kr), (v, vb, vzs, vr)):
            go(remote(src.at[:, head_cols(dz)], buf.at[sp], ss.at[dz], rs.at[sp], sp=dz * n_y + y))
    for off in range(1, n):
        d = lax.rem(sp + off, n)
        dz, dy = d // n_y, lax.rem(d, n_y)
        go(remote(q.at[stripe(dy), head_cols(dz)], qb.at[sp], qs.at[d], qr.at[sp], sp=d))
        go(remote(ft, fb.at[sp], fs.at[d], fr.at[sp], sp=d))

    def weight_slot(item, j):
        if item == 2:
            return db.at[j]
        return (gb, ub)[item].at[pl.ds(pl.multiple_of(j * up_depth, up_depth), up_depth)]

    def weight_up(item, j, d):
        return remote(weight_slot(item, j), weight_slot(item, j), wus.at[item, d], wr.at[item, j], sp=sp + n_y)

    def weight_down(item, j, d):
        return remote(weight_slot(item, j), weight_slot(item, j), wds.at[item, d], wr.at[item, j], sp=sp - n_y)

    def weight_side(item, j, d, oy):
        peer = z * n_y + lax.rem(y + oy, n_y)
        return remote(weight_slot(item, j), weight_slot(item, j), wys.at[item, d, oy], wr.at[item, j], sp=peer)

    def weight_came(item, j):
        weight_up(item, j, 0).wait_recv()

    def pass_on(item, d, act):
        @pl.when(z >= d)
        def _():
            j = sp - d * n_y
            if act == "start":
                weight_came(item, j)

            @pl.when(z < n_z - 1)
            def _():
                getattr(weight_up(item, j, d), act)()

            for oy in range(1, n_y):
                getattr(weight_side(item, j, d, oy), act)()

        @pl.when(z + d < n_z)
        def _():
            j = sp + d * n_y
            if act == "start":
                weight_came(item, j)

            @pl.when(z > 0)
            def _():
                getattr(weight_down(item, j, d), act)()

            for oy in range(1, n_y):
                getattr(weight_side(item, j, n_z - 1 + d, oy), act)()

    def own_lines(item, act):
        @pl.when(z < n_z - 1)
        def _():
            getattr(weight_up(item, sp, 0), act)()

        @pl.when(z > 0)
        def _():
            getattr(weight_down(item, sp, 0), act)()

    def own_sides(item, act):
        for oy in range(1, n_y):
            getattr(weight_side(item, sp, 0, oy), act)()

    for copy in own[4:]:
        copy.wait()
    for item in range(3):
        own_lines(item, "start")

    for copy in own[:4]:
        copy.wait()
    for off in range(n_z):
        src = lax.rem(z + off, n_z) * n_y + y
        for buf, ss, rs in ((kb, kys, kr), (vb, vys, vr)):
            if off:
                remote(buf.at[src], buf.at[src], ss.at[off, 0], rs.at[src], sp=sp).wait_recv()
            for oy in range(1, n_y):
                peer = z * n_y + lax.rem(y + oy, n_y)
                go(remote(buf.at[src], buf.at[src], ss.at[off, oy], rs.at[src], sp=peer))
    for item in range(3):
        own_sides(item, "start")
    for oy in range(1, n_y):
        for zz in range(n_z):
            src = zz * n_y + lax.rem(y + oy, n_y)
            for buf, ss, rs in ((kb, kys, kr), (vb, vys, vr)):
                remote(buf.at[src], buf.at[src], ss.at[0, 0], rs.at[src], sp=sp).wait_recv()
    for off in range(1, n):
        src = lax.rem(sp + off, n)
        remote(qb.at[src], qb.at[src], qs.at[src], qr.at[src], sp=sp).wait_recv()
        remote(fb.at[src], fb.at[src], fs.at[src], fr.at[src], sp=sp).wait_recv()

    pass_on(0, 1, "start")

    head_pick = lax.broadcasted_iota(jnp.int32, fb.shape[1:], 0) == z
    row_id = lax.broadcasted_iota(jnp.int32, (q_rows, rows), 0) + y * q_rows
    col_id = lax.broadcasted_iota(jnp.int32, (q_rows, rows), 1)

    def gate_row(j):
        return jnp.sum(jnp.where(head_pick, fb[j], 0.0), axis=0, keepdims=True)

    def attend(i, unused):
        query = qb[i]
        query_gate = jnp.sum(jnp.where(row_id == col_id, gate_row(i), 0.0), axis=1, keepdims=True)

        def block(j, carried):
            top, total, weighted = carried
            scores = lax.dot_general(
                query, kb[j], (((1,), (1,)), ((), ())), preferred_element_type=F32
            ) * (HD ** -0.5)
            scores = scores + query_gate - gate_row(j)
            scores = jnp.where(col_id + (j - i) * rows <= row_id, scores, -jnp.inf)
            new_top = jnp.maximum(top, jnp.max(scores, axis=1, keepdims=True))
            shrink = jnp.exp(top - new_top)
            expon = jnp.exp(scores - new_top)
            total = shrink * total + jnp.sum(expon, axis=1, keepdims=True)
            weighted = shrink * weighted + jnp.dot(expon.astype(BF16), vb[j], preferred_element_type=F32)
            return new_top, total, weighted

        start = (
            jnp.full((q_rows, 1), -1e30, F32),
            jnp.zeros((q_rows, 1), F32),
            jnp.zeros((q_rows, HD), F32),
        )
        top, total, weighted = lax.fori_loop(0, i + 1, block, start)
        ob[i] = (weighted / total).astype(BF16)
        return unused

    lax.fori_loop(0, n, attend, 0)

    back = pltpu.make_async_copy(ob.at[sp], ab.at[stripe(y), head_cols(z)], local_sem.at[0])
    back.start()
    for off in range(1, n):
        d = lax.rem(sp + off, n)
        go(remote(ob.at[d], ab.at[stripe(y), head_cols(z)], os_.at[d], or_.at[sp], sp=d))
    pass_on(1, 1, "start")
    pass_on(2, 1, "start")
    back.wait()
    for off in range(1, n):
        src = lax.rem(sp + off, n)
        slot = ab.at[stripe(lax.rem(src, n_y)), head_cols(src // n_y)]
        remote(slot, slot, os_.at[src], or_.at[src], sp=sp).wait_recv()

    tile = math.gcd(width, 256)

    def project(c, unused):
        cols = pl.ds(pl.multiple_of(c * tile, tile), tile)
        pb[:, cols] = jnp.dot(ab[...], ow[:, cols], preferred_element_type=F32).astype(BF16)
        return unused

    lax.fori_loop(0, width // tile, project, 0)
    peers = [lax.rem(tp + off, n_tp) for off in range(1, n_tp)]
    for t in peers:
        go(remote(pb.at[tp_rows(t)], rb.at[tp], ps.at[t], pr.at[tp], tp=t))
    pass_on(0, 2, "start")
    for t in peers:
        remote(rb.at[t], rb.at[t], ps.at[t], pr.at[t], tp=tp).wait_recv()
    step = math.gcd(t_rows, 16)

    def normalise(r, unused):
        here = pl.ds(pl.multiple_of(r * step, step), step)
        there = pl.ds(pl.multiple_of(tp * t_rows + r * step, step), step)
        total = pb[there].astype(F32)
        for t in peers:
            total = total + rb[t, here].astype(F32)
        stream = res[here].astype(F32) + total
        st[here] = stream
        mean = jnp.mean(stream * stream, axis=1, keepdims=True)
        xb[there] = (stream * lax.rsqrt(mean + 1e-06) * gain[...].astype(F32)).astype(BF16)
        return unused

    lax.fori_loop(0, t_rows // step, normalise, 0)
    for t in peers:
        go(remote(xb.at[tp_rows(tp)], xb.at[tp_rows(tp)], xs.at[t], xr.at[tp], tp=t))
    pass_on(1, 2, "start")
    pass_on(2, 2, "start")
    for d in range(3, n_z):
        for item in range(3):
            pass_on(item, d, "start")
    for t in peers:
        remote(xb.at[tp_rows(t)], xb.at[tp_rows(t)], xs.at[t], xr.at[t], tp=tp).wait_recv()

    def sides_came(item):
        for zz in range(n_z):
            for oy in range(1, n_y):
                weight_came(item, zz * n_y + lax.rem(y + oy, n_y))

    sides_came(0)
    sides_came(1)
    ffw = gw.shape[1]
    ftile = math.gcd(ffw, 256)

    def widen(c, unused):
        cols = pl.ds(pl.multiple_of(c * ftile, ftile), ftile)
        gate = jnp.dot(xb[...], gb[:, cols], preferred_element_type=F32)
        up = jnp.dot(xb[...], ub[:, cols], preferred_element_type=F32)
        hb[:, cols] = (gate / (1.0 + jnp.exp(-gate)) * up).astype(BF16)
        return unused

    lax.fori_loop(0, ffw // ftile, widen, 0)
    sides_came(2)
    d_cols = dw.shape[1]
    group = max(1, 128 // d_cols)

    def narrow(c, unused):
        parts = [jnp.dot(hb[...], db[c * group + g], preferred_element_type=F32) for g in range(group)]
        joined = parts[0] if group == 1 else jnp.concatenate(parts, axis=1)
        p2[:, pl.ds(pl.multiple_of(c * group * d_cols, group * d_cols), group * d_cols)] = joined.astype(BF16)
        return unused

    lax.fori_loop(0, n // group, narrow, 0)
    for t in peers:
        go(remote(p2.at[tp_rows(t)], r2.at[tp], es.at[t], er.at[tp], tp=t))
    for t in peers:
        remote(r2.at[t], r2.at[t], es.at[t], er.at[t], tp=tp).wait_recv()

    def finish(r, unused):
        here = pl.ds(pl.multiple_of(r * step, step), step)
        there = pl.ds(pl.multiple_of(tp * t_rows + r * step, step), step)
        total = p2[there].astype(F32)
        for t in peers:
            total = total + r2[t, here].astype(F32)
        out[here] = (st[here] + total).astype(BF16)
        return unused

    lax.fori_loop(0, t_rows // step, finish, 0)

    for copy in sends:
        copy.wait_send()
    for item in range(3):
        own_lines(item, "wait_send")
        own_sides(item, "wait_send")
        for d in range(1, n_z):
            pass_on(item, d, "wait_send")


def shards(n, n_tp, q, k, v, forget_sums, residual_in, out_weight, norm_gain, gate_weight, up_weight, down_weight):
    rows, wide = q.shape
    heads = wide // HD
    n_y = n // heads
    q_rows, t_rows, width = rows // n_y, rows // n_tp, out_weight.shape[1]
    ffw, d_cols = gate_weight.shape[1], down_weight.shape[1]
    lanes = -(-heads // 8) * 8
    ft = jnp.pad(forget_sums.T, ((0, lanes - heads), (0, 0)))
    dma = lambda *shape: pltpu.SemaphoreType.DMA(shape)
    scratch = [
        pltpu.VMEM((n, q_rows, HD), BF16),
        pltpu.VMEM((n, rows, HD), BF16),
        pltpu.VMEM((n, rows, HD), BF16),
        pltpu.VMEM((n, lanes, rows), F32),
        pltpu.VMEM((n, q_rows, HD), BF16),
        pltpu.VMEM((rows, wide), BF16),
        pltpu.VMEM((rows, width), BF16),
        pltpu.VMEM((n_tp, t_rows, width), BF16),
        pltpu.VMEM((t_rows, width), F32),
        pltpu.VMEM((rows, width), BF16),
        pltpu.VMEM((width, ffw), BF16),
        pltpu.VMEM((width, ffw), BF16),
        pltpu.VMEM((n, ffw, d_cols), BF16),
        pltpu.VMEM((rows, ffw), BF16),
        pltpu.VMEM((rows, width), BF16),
        pltpu.VMEM((n_tp, t_rows, width), BF16),
        dma(7), dma(n), dma(n), dma(n), dma(n),
        dma(heads), dma(heads, n_y), dma(n), dma(heads), dma(heads, n_y), dma(n),
        dma(3, heads), dma(3, heads), dma(3, 2 * heads, n_y), dma(3, n),
        dma(n), dma(n), dma(n_tp), dma(n_tp), dma(n_tp), dma(n_tp), dma(n_tp), dma(n_tp),
    ]
    vmem = pl.BlockSpec(memory_space=pltpu.VMEM)
    return pl.pallas_call(
        functools.partial(layer_kernel, n, n_tp, heads),
        out_shape=jax.ShapeDtypeStruct((t_rows, width), BF16),
        in_specs=[vmem] * 10,
        out_specs=vmem,
        scratch_shapes=scratch,
        compiler_params=pltpu.CompilerParams(has_side_effects=True, vmem_limit_bytes=60 * 1024 * 1024),
    )(q, k, v, ft, residual_in, out_weight, norm_gain.reshape(1, -1), gate_weight, up_weight, down_weight)


def solution(mesh):
    placed = (
        P("sp", "tp"),
        P("sp", "tp"),
        P("sp", "tp"),
        P("sp", "tp"),
        P(("sp", "tp"), None),
        P("tp", None),
        P(),
        P("sp", "tp"),
        P("sp", "tp"),
        P("tp", "sp"),
    )
    return jax.shard_map(
        functools.partial(shards, mesh.shape["sp"], mesh.shape["tp"]),
        mesh=mesh, in_specs=placed, out_specs=P(("sp", "tp"), None), check_vma=False,
    )
```

time: 442 us -> 182 us (0.41)
  waiting for transfers between devices: 354 us -> 0 us
  Pallas kernels: 0 us -> 177 us
  matrix products: 30.1 us -> 0 us
  blocking collectives: 23.1 us -> 0 us
  between operations: 13.6 us -> 0.01 us
  other arithmetic: 9.88 us -> 0 us
    all_gather x6 -> x0, waiting for transfers between devices: 295 us -> none  [the longest x1 62.3 us: shards(): lax.all_gather(down_weight, 'sp', axis=1, tiled=True)]
    pallas_call x0 -> x1, Pallas kernels: none -> 177 us  [shards(): pl.pallas_call(functools.partial(layer_kernel, n, n_tp, heads), out_shape...]
    reduce_scatter x2 -> x0, waiting for transfers between devices: 56.3 us -> none  [the longest x1 28.8 us: shards(): lax.psum_scatter(partial_value.astype(jnp.float32).astype(jnp.bfloat16),...]
    dot_general x51 -> x0, matrix products: 30.1 us -> none  [the longest x24 8.28 us: attend_block(): jnp.einsum('qd,kd->qk', query_rows[:, columns], key_rows[:, columns], pre...]
    all_gather x1 -> x0, blocking collectives: 23.1 us -> none  [shards(): all_gates = lax.all_gather(forget_sums, 'sp', axis=0, tiled=True)]
    squeeze x12 -> x0, local copies, waits for them, and re-layouts: 7.7 us -> none  [shards(): carried, unused = lax.scan(advance, carried, blocks)]
    reduce_sum x25 -> x0, other arithmetic: 5.03 us -> none  [the longest x24 3.81 us: attend_block(): totals.append(shrink * row_total[:, head_index] + jnp.sum(expon, axis=1))]
  transfers between devices with their start and end apart: 8 -> 0, of which waited for: 8 -> 0; matrix products, arithmetic and copies ran while one was open for 2% -> 0% of each run, Pallas kernels for 0% -> 0%
where the time goes in v1:
time: 182 us
  Pallas kernels  177 us (97%)
  local copies, waits for them, and re-layouts  4.35 us (2%)
    pallas_call x1, Pallas kernels, shards(): pl.pallas_call(functools.partial(layer_kernel, n, n_tp, heads), out_shape...  177 us

profile of v1, /device:TPU:9, one launch (start us, length us, event | category | flops | bytes accessed | tf_op | source)
XLA Modules:
  0.0 181.8 jit_solution(1268348155917180118)
XLA Ops:
  0.0 1.3 reshape.3.gain
  1.3 1.3 pad.4.ft
  2.6 177.4 %shard_map.100 = bf16[96,2048]{1,0:T(8,128)(2,1)} custom-call(bf16[384,512]{1,0:T(8,128)(2,1)} %q.1, bf16[384,512]{1,0:T(8,128)(2,1)} %k.1, bf16[384,512]{1,0:T(8,128)(2,1)} %v.1, f32[8,384]{1,0:T(8,128)} %pad.4.ft, bf16[96,2048]{1,0:T(8,128)(2,1)} %res.1, bf16[512,2048]{1,0:T(8,128)(2,1)} %ow.1, bf16[1,2048]{1,0:T(2,128)(2,1)} %reshape.3.gain, ...), custom_call_target="tpu_custom_call" | custom-call | tf_op jit(solution)/shard_map/pallas_call | solution.py:343
  180.0 1.8 copy.12

commit v2 on v1

--- a/solution.py
+++ b/solution.py
@@ -28,9 +28,9 @@
     n, n_tp, heads,
     q, k, v, ft, res, ow, gain, gw, uw, dw,
     out,
-    qb, kb, vb, fb, ob, ab, pb, rb, st, xb, gb, ub, db, hb, p2, r2,
+    qb, kb, vb, fb, ob, ab, pb, s1, s2, st, xb, gb, ub, db, hb, p2, e1, e2,
     local_sem, qs, qr, fs, fr, kzs, kys, kr, vzs, vys, vr,
-    wus, wds, wys, wr, os_, or_, ps, pr, xs, xr, es, er,
+    wus, wds, wys, wr, aus, ads, ays, ar, os_, or_, ps, pr, p2s, p2r, xs, xr, xf, es, er, e2s, e2r,
 ):
     sp, tp = lax.axis_index("sp"), lax.axis_index("tp")
     n_z = heads
@@ -79,9 +79,11 @@
         go(remote(q.at[stripe(dy), head_cols(dz)], qb.at[sp], qs.at[d], qr.at[sp], sp=d))
         go(remote(ft, fb.at[sp], fs.at[d], fr.at[sp], sp=d))
 
+    half = dw.shape[0] // 2
+
     def weight_slot(item, j):
         if item == 2:
-            return db.at[j]
+            return db.at[j, :half]
         return (gb, ub)[item].at[pl.ds(pl.multiple_of(j * up_depth, up_depth), up_depth)]
 
     def weight_up(item, j, d):
@@ -136,6 +138,40 @@
     def own_sides(item, act):
         for oy in range(1, n_y):
             getattr(weight_side(item, sp, 0, oy), act)()
+
+    def late_copy(j, send_sem, peer):
+        return remote(db.at[j, half:], db.at[j, half:], send_sem, ar.at[j], sp=peer)
+
+    def late_came(j):
+        late_copy(j, aus.at[0, 0], sp).wait_recv()
+
+    def late_sides(act):
+        for oy in range(1, n_y):
+            getattr(late_copy(sp, ays.at[oy], z * n_y + lax.rem(y + oy, n_y)), act)()
+
+    def late_lines(d, act):
+        for oy in range(n_y):
+            column = lax.rem(y + oy, n_y)
+
+            below, above = (z - d) * n_y + column, (z + d) * n_y + column
+            if act == "start" and (d or oy):
+                @pl.when(z >= d)
+                def _():
+                    late_came(below)
+
+            if act == "start" and d:
+                @pl.when(z + d < n_z)
+                def _():
+                    late_came(above)
+
+            if d < n_z - 1:
+                @pl.when(jnp.minimum(z - d, n_z - 2 - z) >= 0)
+                def _():
+                    getattr(late_copy(below, aus.at[d, oy], sp + n_y), act)()
+
+                @pl.when(jnp.minimum(z - 1, n_z - 1 - d - z) >= 0)
+                def _():
+                    getattr(late_copy(above, ads.at[d, oy], sp - n_y), act)()
 
     for copy in own[4:]:
         copy.wait()
@@ -152,6 +188,7 @@
             for oy in range(1, n_y):
                 peer = z * n_y + lax.rem(y + oy, n_y)
                 go(remote(buf.at[src], buf.at[src], ss.at[off, oy], rs.at[src], sp=peer))
+    late_sides("start")
     for item in range(3):
         own_sides(item, "start")
     for oy in range(1, n_y):
@@ -163,8 +200,6 @@
         src = lax.rem(sp + off, n)
         remote(qb.at[src], qb.at[src], qs.at[src], qr.at[src], sp=sp).wait_recv()
         remote(fb.at[src], fb.at[src], fs.at[src], fr.at[src], sp=sp).wait_recv()
-
-    pass_on(0, 1, "start")
 
     head_pick = lax.broadcasted_iota(jnp.int32, fb.shape[1:], 0) == z
     row_id = lax.broadcasted_iota(jnp.int32, (q_rows, rows), 0) + y * q_rows
@@ -207,8 +242,8 @@
     for off in range(1, n):
         d = lax.rem(sp + off, n)
         go(remote(ob.at[d], ab.at[stripe(y), head_cols(z)], os_.at[d], or_.at[sp], sp=d))
-    pass_on(1, 1, "start")
-    pass_on(2, 1, "start")
+    for item in range(3):
+        pass_on(item, 1, "start")
     back.wait()
     for off in range(1, n):
         src = lax.rem(sp + off, n)
@@ -223,36 +258,100 @@
         return unused
 
     lax.fori_loop(0, width // tile, project, 0)
-    peers = [lax.rem(tp + off, n_tp) for off in range(1, n_tp)]
-    for t in peers:
-        go(remote(pb.at[tp_rows(t)], rb.at[tp], ps.at[t], pr.at[tp], tp=t))
-    pass_on(0, 2, "start")
-    for t in peers:
-        remote(rb.at[t], rb.at[t], ps.at[t], pr.at[t], tp=tp).wait_recv()
+    n_c = 2 if n_tp % 2 == 0 else 1
+    n_a = n_tp // n_c
+    a_here, c_here = tp // n_c, lax.rem(tp, n_c)
+    a_peers = [lax.rem(a_here + off, n_a) for off in range(1, n_a)]
+    c_peers = [lax.rem(c_here + off, n_c) for off in range(1, n_c)]
     step = math.gcd(t_rows, 16)
+
+    def near_sends(part, near, ss, rs):
+        for a in a_peers + [a_here]:
+            for c in c_peers:
+                go(remote(part.at[tp_rows(a * n_c + c)], near.at[c_here, a], ss.at[a, c], rs.at[c_here, a],
+                          tp=a_here * n_c + c))
+
+    def near_wait(near, a, ss, rs):
+        for c in c_peers:
+            remote(near.at[c, a], near.at[c, a], ss.at[a, c], rs.at[c, a], tp=tp).wait_recv()
+
+    def far_sends(part, near, far, ss, rs, far_ss, far_rs):
+        for a in a_peers:
+            near_wait(near, a, ss, rs)
+
+            def add(r, unused, a=a):
+                here = pl.ds(pl.multiple_of(r * step, step), step)
+                there = pl.ds(pl.multiple_of((a * n_c + c_here) * t_rows + r * step, step), step)
+                total = part[there].astype(F32)
+                for c in c_peers:
+                    total = total + near[c, a, here].astype(F32)
+                part[there] = total.astype(BF16)
+                return unused
+
+            lax.fori_loop(0, t_rows // step, add, 0)
+        for a in a_peers:
+            go(remote(part.at[tp_rows(a * n_c + c_here)], far.at[a_here], far_ss.at[a], far_rs.at[a_here],
+                      tp=a * n_c + c_here))
+
+    def far_wait(near, far, ss, rs, far_ss, far_rs):
+        near_wait(near, a_here, ss, rs)
+        for a in a_peers:
+            remote(far.at[a], far.at[a], far_ss.at[a], far_rs.at[a], tp=tp).wait_recv()
+
+    def summed(part, near, far, here, there):
+        total = part[there].astype(F32)
+        for c in c_peers:
+            total = total + near[c, a_here, here].astype(F32)
+        for a in a_peers:
+            total = total + far[a, here].astype(F32)
+        return total
+
+    near_sends(pb, s1, ps, pr)
+    far_sends(pb, s1, s2, ps, pr, p2s, p2r)
+    for item in range(3):
+        pass_on(item, 2, "start")
+    late_lines(0, "start")
+    far_wait(s1, s2, ps, pr, p2s, p2r)
 
     def normalise(r, unused):
         here = pl.ds(pl.multiple_of(r * step, step), step)
         there = pl.ds(pl.multiple_of(tp * t_rows + r * step, step), step)
-        total = pb[there].astype(F32)
-        for t in peers:
-            total = total + rb[t, here].astype(F32)
-        stream = res[here].astype(F32) + total
+        stream = res[here].astype(F32) + summed(pb, s1, s2, here, there)
         st[here] = stream
         mean = jnp.mean(stream * stream, axis=1, keepdims=True)
         xb[there] = (stream * lax.rsqrt(mean + 1e-06) * gain[...].astype(F32)).astype(BF16)
         return unused
 
     lax.fori_loop(0, t_rows // step, normalise, 0)
-    for t in peers:
-        go(remote(xb.at[tp_rows(tp)], xb.at[tp_rows(tp)], xs.at[t], xr.at[tp], tp=t))
-    pass_on(1, 2, "start")
-    pass_on(2, 2, "start")
+    def rows_to(t_src, t_dst, ss):
+        return remote(xb.at[tp_rows(t_src)], xb.at[tp_rows(t_src)], ss, xr.at[t_src], tp=t_dst)
+
+    for a in a_peers:
+        go(rows_to(tp, a * n_c + c_here, xs.at[a * n_c + c_here]))
+    for c in c_peers:
+        go(rows_to(tp, a_here * n_c + c, xs.at[a_here * n_c + c]))
+    if n_z > 3:
+        pass_on(0, 3, "start")
+    for a in a_peers:
+        t = a * n_c + c_here
+        rows_to(t, tp, xs.at[t]).wait_recv()
+        for c in c_peers:
+            go(rows_to(t, a_here * n_c + c, xf.at[a, c]))
     for d in range(3, n_z):
         for item in range(3):
-            pass_on(item, d, "start")
-    for t in peers:
-        remote(xb.at[tp_rows(t)], xb.at[tp_rows(t)], xs.at[t], xr.at[t], tp=tp).wait_recv()
+            if (item, d) != (0, 3):
+                if item == 2 and d == 3:
+                    late_lines(1, "start")
+                pass_on(item, d, "start")
+    if n_z <= 3:
+        late_lines(1, "start")
+    for d in range(2, n_z):
+        if d < n_z - 1:
+            late_lines(d, "start")
+    for a in range(n_a):
+        for c in c_peers:
+            t = a * n_c + c
+            rows_to(t, tp, xs.at[t]).wait_recv()
 
     def sides_came(item):
         for zz in range(n_z):
@@ -273,6 +372,7 @@
 
     lax.fori_loop(0, ffw // ftile, widen, 0)
     sides_came(2)
+    late_lines(n_z - 1, "start")
     d_cols = dw.shape[1]
     group = max(1, 128 // d_cols)
 
@@ -283,18 +383,14 @@
         return unused
 
     lax.fori_loop(0, n // group, narrow, 0)
-    for t in peers:
-        go(remote(p2.at[tp_rows(t)], r2.at[tp], es.at[t], er.at[tp], tp=t))
-    for t in peers:
-        remote(r2.at[t], r2.at[t], es.at[t], er.at[t], tp=tp).wait_recv()
+    near_sends(p2, e1, es, er)
+    far_sends(p2, e1, e2, es, er, e2s, e2r)
+    far_wait(e1, e2, es, er, e2s, e2r)
 
     def finish(r, unused):
         here = pl.ds(pl.multiple_of(r * step, step), step)
         there = pl.ds(pl.multiple_of(tp * t_rows + r * step, step), step)
-        total = p2[there].astype(F32)
-        for t in peers:
-            total = total + r2[t, here].astype(F32)
-        out[here] = (st[here] + total).astype(BF16)
+        out[here] = (st[here] + summed(p2, e1, e2, here, there)).astype(BF16)
         return unused
 
     lax.fori_loop(0, t_rows // step, finish, 0)
@@ -306,6 +402,9 @@
         own_sides(item, "wait_send")
         for d in range(1, n_z):
             pass_on(item, d, "wait_send")
+    late_sides("wait_send")
+    for d in range(n_z):
+        late_lines(d, "wait_send")
 
 
 def shards(n, n_tp, q, k, v, forget_sums, residual_in, out_weight, norm_gain, gate_weight, up_weight, down_weight):
@@ -314,6 +413,8 @@
     n_y = n // heads
     q_rows, t_rows, width = rows // n_y, rows // n_tp, out_weight.shape[1]
     ffw, d_cols = gate_weight.shape[1], down_weight.shape[1]
+    n_c = 2 if n_tp % 2 == 0 else 1
+    n_a = n_tp // n_c
     lanes = -(-heads // 8) * 8
     ft = jnp.pad(forget_sums.T, ((0, lanes - heads), (0, 0)))
     dma = lambda *shape: pltpu.SemaphoreType.DMA(shape)
@@ -325,7 +426,8 @@
         pltpu.VMEM((n, q_rows, HD), BF16),
         pltpu.VMEM((rows, wide), BF16),
         pltpu.VMEM((rows, width), BF16),
-        pltpu.VMEM((n_tp, t_rows, width), BF16),
+        pltpu.VMEM((n_c, n_a, t_rows, width), BF16),
+        pltpu.VMEM((n_a, t_rows, width), BF16),
         pltpu.VMEM((t_rows, width), F32),
         pltpu.VMEM((rows, width), BF16),
         pltpu.VMEM((width, ffw), BF16),
@@ -333,11 +435,14 @@
         pltpu.VMEM((n, ffw, d_cols), BF16),
         pltpu.VMEM((rows, ffw), BF16),
         pltpu.VMEM((rows, width), BF16),
-        pltpu.VMEM((n_tp, t_rows, width), BF16),
+        pltpu.VMEM((n_c, n_a, t_rows, width), BF16),
+        pltpu.VMEM((n_a, t_rows, width), BF16),
         dma(7), dma(n), dma(n), dma(n), dma(n),
         dma(heads), dma(heads, n_y), dma(n), dma(heads), dma(heads, n_y), dma(n),
         dma(3, heads), dma(3, heads), dma(3, 2 * heads, n_y), dma(3, n),
-        dma(n), dma(n), dma(n_tp), dma(n_tp), dma(n_tp), dma(n_tp), dma(n_tp), dma(n_tp),
+        dma(heads, n_y), dma(heads, n_y), dma(n_y), dma(n),
+        dma(n), dma(n), dma(n_a, n_c), dma(n_c, n_a), dma(n_a), dma(n_a),
+        dma(n_tp), dma(n_tp), dma(n_a, n_c), dma(n_a, n_c), dma(n_c, n_a), dma(n_a), dma(n_a),
     ]
     vmem = pl.BlockSpec(memory_space=pltpu.VMEM)
     return pl.pallas_call(

time: 182 us -> 163 us (0.90)
  Pallas kernels: 177 us -> 159 us
    pallas_call x1, Pallas kernels: 177 us -> 159 us  [shards(): pl.pallas_call(functools.partial(layer_kernel, n, n_tp, heads), out_shape...]
where the time goes in v2:
time: 163 us
  Pallas kernels  159 us (98%)
  local copies, waits for them, and re-layouts  4.35 us (3%)
    pallas_call x1, Pallas kernels, shards(): pl.pallas_call(functools.partial(layer_kernel, n, n_tp, heads), out_shape...  159 us

profile of v2, /device:TPU:9, one launch (start us, length us, event | category | flops | bytes accessed | tf_op | source)
XLA Modules:
  0.0 163.1 jit_solution(4933671128365430023)
XLA Ops:
  0.0 1.3 reshape.3.gain
  1.3 1.3 pad.4.ft
  2.6 158.7 %shard_map.100 = bf16[96,2048]{1,0:T(8,128)(2,1)} custom-call(bf16[384,512]{1,0:T(8,128)(2,1)} %q.1, bf16[384,512]{1,0:T(8,128)(2,1)} %k.1, bf16[384,512]{1,0:T(8,128)(2,1)} %v.1, f32[8,384]{1,0:T(8,128)} %pad.4.ft, bf16[96,2048]{1,0:T(8,128)(2,1)} %res.1, bf16[512,2048]{1,0:T(8,128)(2,1)} %ow.1, bf16[1,2048]{1,0:T(2,128)(2,1)} %reshape.3.gain, ...), custom_call_target="tpu_custom_call" | custom-call | tf_op jit(solution)/shard_map/pallas_call | solution.py:448
  161.3 1.8 %copy.12 = bf16[96,2048]{1,0:T(8,128)(2,1)} copy(bf16[96,2048]{1,0:T(8,128)(2,1)} %shard_map.100) | data formatting | bytes 786432
